TPU v7x, 512 devices: a whole 4x4x16 slice. The times are simulated.
512 devices in a mesh: sp: 64 (over z, y), tp: 8 (over x, core).
Axes of the slice: x: 4, y: 4, z: 16, core: 2. Of those that a mesh axis runs over, the one named last changes fastest.
Arguments:
- tokens: bfloat16 [8192, 1024], P('sp', 'tp'), may hold values from -6 to 6
- norm_gain: float32 [1024], P('tp'), may hold values from 0.1 to 1.9
- query_weight: bfloat16 [1024, 1024], P('sp', 'tp'), may hold values from -0.1875 to 0.1875
- key_weight: bfloat16 [1024, 512], P('sp', 'tp'), may hold values from -0.1875 to 0.1875
- value_weight: bfloat16 [1024, 512], P('sp', 'tp'), may hold values from -0.1875 to 0.1875
- conv_in_weight: bfloat16 [1024, 1024], P('sp', 'tp'), may hold values from -0.1875 to 0.1875
- pre_weight: bfloat16 [1024, 1024], P('sp', 'tp'), may hold values from -0.1875 to 0.1875
- post_weight: bfloat16 [1024, 1024], P('sp', 'tp'), may hold values from -0.1875 to 0.1875
- attn_gate_weight: bfloat16 [1024, 1024], P('sp', 'tp'), may hold values from -0.1875 to 0.1875
- conv_gate_weight: bfloat16 [1024, 1024], P('sp', 'tp'), may hold values from -0.1875 to 0.1875
- sink_logit: float32 [16], P('tp'), may hold values from 1 to 5
- conv_taps: float32 [3, 1024], P(None, 'tp'), may hold values from -3 to 3
- attn_out_weight: bfloat16 [1024, 1024], P('tp', 'sp'), may hold values from -1 to 1
- conv_out_weight: bfloat16 [1024, 1024], P('tp', 'sp'), may hold values from -0.1875 to 0.1875
Outputs:
- merged: bfloat16 [8192, 1024], P('sp', 'tp')
All inputs are finite; a program needn't handle non-finite values.
Results may differ from a plain program's by a relative error of at most 0.003.
Values may be sent and summed in bfloat16 or wider, within the bound.
A program may use at most 64 MiB of HBM per device.

v0:
```python
import jax
import jax.numpy as jnp
from jax import lax
from jax.sharding import Mesh
from jax.sharding import PartitionSpec as P

HEAD_DIM = 64
WINDOW = 64
TP = ("tp_0", "tp_1")


epsilon = 1e-06
negative = -1e30


def gathered_total(shard, axis):
    blocks = lax.all_gather(shard, axis)
    return blocks.sum(axis=0)


def joined_along(blocks, dim):
    blocks = jnp.moveaxis(blocks, 0, dim)
    lengths = blocks.shape
    return blocks.reshape(*lengths[:dim], lengths[dim] * lengths[dim + 1], *lengths[dim + 2 :])


def gather_packed(arrays, axis, dims):
    flat = jnp.concatenate([a.reshape(-1) for a in arrays])
    lines, at, finished = lax.all_gather(flat, axis), 0, []
    for a, dim in zip(arrays, dims):
        blocks = lines[:, at : at + a.size].reshape(-1, *a.shape)
        finished.append(joined_along(blocks, dim))
        at += a.size
    return tuple(finished)


def gather_axes(shard, axes, dim):
    for axis in reversed(axes):
        shard = lax.all_gather(shard, axis, axis=dim, tiled=True)
    return shard


def folded(shard, axes, dim, update, carry):
    everything = jax.tree.map(lambda part: gather_axes(part, axes, dim), shard)
    return update(carry, everything, jnp.int32(0))


def shortened(shard):
    def short(part):
        return part.astype(jnp.bfloat16) if part.dtype == jnp.float32 else part

    return jax.tree.map(short, shard)


def padded_2(shard, sides, width, wrap):
    for axis, dim in sides:
        devices, length = lax.axis_size(axis), shard.shape[dim]
        up = [(i, (i + 1) % devices) for i in range(devices if wrap else devices - 1)]
        down = [(j, i) for i, j in up]
        last = lax.slice_in_dim(shard, length - width, length, axis=dim)
        first = lax.slice_in_dim(shard, 0, width, axis=dim)
        before = lax.ppermute(last, axis, up)
        after = lax.ppermute(first, axis, down)
        shard = jnp.concatenate([before, shard, after], axis=dim)
    return shard


def scattered(portion, width, axis):
    count = width * lax.axis_size(axis)
    return lax.psum_scatter(portion(jnp.int32(0), count), axis, scatter_dimension=0, tiled=True)


def window_mix(queries, key_rows, value_rows, sink_cols, first, seq_total):
    score_scale = queries.shape[-1] ** (-0.5)
    scores = (
        jnp.einsum("qhgd,khd->hgqk", queries, key_rows, preferred_element_type=jnp.float32)
        * score_scale
    )
    qpos = first + jnp.arange(queries.shape[0], dtype=jnp.int32)
    kpos = first - WINDOW + jnp.arange(key_rows.shape[0], dtype=jnp.int32)
    allowed = (
        (jnp.abs(qpos[:, None] - kpos[None, :]) <= WINDOW)
        & (kpos >= 0)[None, :]
        & (kpos < seq_total)[None, :]
    )
    scores = jnp.where(allowed, scores, negative)
    column = jnp.broadcast_to(sink_cols[:, :, None, None], scores.shape[:-1] + (1,))
    weights_soft = jax.nn.softmax(jnp.concatenate([scores, column], axis=-1), axis=-1)[..., :-1]
    return jnp.einsum(
        "hgqk,khd->qhgd",
        weights_soft,
        value_rows.astype(jnp.float32),
        precision=lax.Precision.HIGHEST,
    )


def short_conv(padded, conv_taps):
    return (
        conv_taps[0][None, :] * padded[:-2]
        + conv_taps[1][None, :] * padded[1:-1]
        + conv_taps[2][None, :] * padded[2:]
    )


def on_device(
    tokens,
    norm_gain,
    query_weight,
    key_weight,
    value_weight,
    conv_in_weight,
    pre_weight,
    post_weight,
    attn_gate_weight,
    conv_gate_weight,
    sink_logit,
    conv_taps,
    attn_out_weight,
    conv_out_weight,
):
    tok_rows = tokens.shape[0]
    widened = tokens.astype(jnp.float32)
    row_sums = gathered_total(jnp.sum(widened * widened, axis=1), TP)
    features = tokens.shape[1] * lax.axis_size(TP)
    normed = (
        widened * lax.rsqrt(row_sums[:, None] / features + epsilon) * norm_gain[None, :]
    ).astype(jnp.bfloat16)
    collected = gather_packed(
        (
            query_weight,
            key_weight,
            value_weight,
            conv_in_weight,
            pre_weight,
            post_weight,
            attn_gate_weight,
            conv_gate_weight,
        ),
        "sp",
        (0, 0, 0, 0, 0, 0, 0, 0),
    )
    stacked = jnp.concatenate(collected, axis=1)

    def add_rows(carry_sum, segment, first):
        rows_here = lax.dynamic_slice_in_dim(stacked, first, segment.shape[1], 0)
        return carry_sum + jnp.dot(segment, rows_here, preferred_element_type=jnp.float32)

    projected = folded(
        normed, TP, 1, add_rows, jnp.zeros((tok_rows, stacked.shape[1]), jnp.float32)
    )
    pieces = []
    offset = 0
    for weight in collected:
        pieces.append(projected[:, offset : offset + weight.shape[1]])
        offset = offset + weight.shape[1]
    queries, key_rows, value_rows, conv_in, pre_gate, post_gate = [
        part_rows.astype(jnp.bfloat16) for part_rows in pieces[:6]
    ]
    attn_gate = pieces[6]
    conv_gate = pieces[7]
    conv_mix = (pre_gate.astype(jnp.float32) * conv_in.astype(jnp.float32)).astype(jnp.bfloat16)
    kv_width = key_rows.shape[1]
    padded = padded_2(
        shortened(jnp.concatenate([key_rows, value_rows, conv_mix], axis=1)),
        (("sp", 0),),
        WINDOW,
        False,
    )
    key_pad = padded[:, :kv_width]
    value_pad = padded[:, kv_width : 2 * kv_width]
    conv_pad = padded[WINDOW - 1 : WINDOW + tok_rows + 1, 2 * kv_width :]
    kv_local = kv_width // HEAD_DIM
    group_size = queries.shape[1] // kv_width
    first_row = lax.axis_index("sp") * tok_rows
    attended = window_mix(
        queries.reshape(tok_rows, kv_local, group_size, HEAD_DIM),
        key_pad.reshape(-1, kv_local, HEAD_DIM),
        value_pad.reshape(-1, kv_local, HEAD_DIM),
        sink_logit.reshape(kv_local, group_size),
        first_row,
        tok_rows * lax.axis_size("sp"),
    )
    attended = attended.reshape(tok_rows, -1).astype(jnp.bfloat16)
    conv_out = (
        post_gate.astype(jnp.float32) * short_conv(conv_pad.astype(jnp.float32), conv_taps)
    ).astype(jnp.bfloat16)
    attn_full, conv_full = gather_packed((attn_out_weight, conv_out_weight), "sp", (1, 1))

    def attn_term(first, number):
        columns = lax.dynamic_slice_in_dim(attn_full, first, number, 1)
        return jnp.dot(attended, columns, preferred_element_type=jnp.float32).T

    def conv_term(first, number):
        columns = lax.dynamic_slice_in_dim(conv_full, first, number, 1)
        return jnp.dot(conv_out, columns, preferred_element_type=jnp.float32).T

    out_rows = attn_gate.shape[1]

    def both_terms(first, number):
        return jnp.concatenate([attn_term(first, number), conv_term(first, number)], axis=1)

    summed = scattered(both_terms, out_rows, TP)
    branch_attn = summed[:, :tok_rows].T
    branch_conv = summed[:, tok_rows:].T
    return (
        jax.nn.sigmoid(attn_gate) * branch_attn + jax.nn.sigmoid(conv_gate) * branch_conv
    ).astype(jnp.bfloat16)


def solution(mesh):
    finer = Mesh(mesh.devices.reshape(mesh.shape["sp"], 4, 2), ("sp", "tp_0", "tp_1"))
    return jax.shard_map(
        on_device,
        mesh=finer,
        in_specs=(
            P("sp", TP),
            P(TP),
            P("sp", TP),
            P("sp", TP),
            P("sp", TP),
            P("sp", TP),
            P("sp", TP),
            P("sp", TP),
            P("sp", TP),
            P("sp", TP),
            P(TP),
            P(None, TP),
            P(TP, "sp"),
            P(TP, "sp"),
        ),
        out_specs=P("sp", TP),
        check_vma=False,
    )
```

profile of v0, /device:TPU:1, one launch (start us, length us, event | category | flops | bytes accessed | tf_op | source)
XLA Modules:
  0.0 228.6 jit_solution(1627320652116977208)
XLA Ops:
  6.5 0.7 constant_dynamic-update-slice_fusion.7
  7.3 0.8 reshape.161
  8.0 0.8 reshape.162
  8.8 0.7 constant_dynamic-update-slice_fusion.4
  9.5 0.7 constant_dynamic-update-slice_fusion.3
  10.2 0.7 constant_dynamic-update-slice_fusion.2
  10.9 0.7 constant_dynamic-update-slice_fusion.1
  11.6 0.7 constant_dynamic-update-slice_fusion
  12.9 0.8 copy.37
  13.8 0.8 copy.38
  14.7 84.0 %all-gather.2 = bf16[262144]{0:T(1024)(128)(2,1)S(1)} all-gather(bf16[4096]{0:T(1024)(128)(2,1)S(1)} %pad_maximum_fusion.3), channel_id=4, replica_groups=mesh['sp'=64,'tp_0'=4,'tp_1'=2] {'sp'}, dimensions={0}, use_global_device_ids=true | all-gather | bytes 532480 | tf_op jit(solution)/shard_map/all_gather | solution.py:29
  99.1 34.9 %all-gather.3 = f32[8,1,128]{2,1,0:T(1,128)S(1)} all-gather(f32[1,1,128]{2,1,0:T(1,128)S(1)} %bitcast.76), channel_id=2, replica_groups=mesh['sp'=64,'tp_0'=4,'tp_1'=2] {'tp_0','tp_1'}, dimensions={0}, use_global_device_ids=true | all-gather | bytes 4608 | tf_op jit(solution)/shard_map/all_gather | solution.py:17
  134.2 1.9 all_gather.26
  136.0 11.0 %all_gather.27 = bf16[128,1024]{1,0:T(8,128)(2,1)} all-gather(bf16[128,256]{1,0:T(8,128)(2,1)S(1)} %all_gather.26), channel_id=1, replica_groups=mesh['sp'=64,'tp_0'=4,'tp_1'=2] {'tp_0'}, dimensions={1}, use_global_device_ids=true | all-gather | bytes 327680 | tf_op jit(solution)/shard_map/all_gather | solution.py:39
  147.0 0.8 fusion.7
  147.8 0.8 fusion.37
  149.3 2.6 %reshape.177 = bf16[64,14336]{1,0:T(8,128)(2,1)S(1)} reshape(bf16[917504]{0:T(1024)(128)(2,1)} %all-gather.6.cloned.1.call-done) | data formatting | bytes 3670016 | tf_op jit(solution)/shard_map/all_gather | solution.py:29
  152.1 0.7 fusion.36
  152.8 0.8 reshape_reshape.24
  153.6 0.8 reshape_reshape.27
  154.4 0.8 reshape_reshape.28
  155.4 0.8 reshape_reshape.30
  156.2 0.8 reshape_reshape.31
  157.2 0.9 reshape_reshape.26
  158.1 2.3 concatenate.34
  160.5 1.2 fusion.39
  161.8 2.4 %collective-permute-start = (bf16[64,256]{1,0:T(8,128)(2,1)S(1)}, bf16[64,256]{1,0:T(8,128)(2,1)S(1)}, u32[]{:S(2)}, u32[]{:S(2)}) collective-permute-start(bf16[64,256]{1,0:T(8,128)(2,1)S(1)} %get-tuple-element.19), channel_id=1, source_target_pairs={{0,8},{8,16},{16,24},{24,32},{32,40},{40,48},{48,56},{56,64},{64,7... | collective-permute-start | bytes 98312 | tf_op jit(solution)/shard_map/ppermute | solution.py:62
  164.1 1.3 collective-permute-start.1
  167.4 1.4 collective-permute-done.1
  170.1 1.0 pad_maximum_fusion
  171.1 49.0 %reduce-scatter.2.cloned.1.call-done = f32[128,256]{0,1:T(8,128)} async-done(((f32[1024,256]{0,1:T(8,128)}), f32[128,256]{0,1:T(8,128)}) %reduce-scatter.2.cloned.1.call-update) | async-done | bytes 131088 | tf_op jit(solution)/shard_map/reduce_scatter | solution.py:70
  220.2 1.6 fusion.13
  (66 shorter events, 5.6 us)
Async XLA Ops:
  6.5 92.4 %copy-start.7 = (bf16[128,128]{1,0:T(8,128)(2,1)S(1)}, bf16[128,128]{1,0:T(8,128)(2,1)}, u32[]{:S(2)}) copy-start(bf16[128,128]{1,0:T(8,128)(2,1)} %param.14) | copy-start | bytes 98308
  6.5 127.5 %copy-start.11 = (f32[128]{0:T(128)S(1)}, f32[128]{0:T(128)}, u32[]{:S(2)}) copy-start(f32[128]{0:T(128)} %param.15) | copy-start | bytes 1540
  6.5 142.7 %all-gather.6.cloned.1.call-start = ((), (), s32[]{:S(2)}) async-start(), calls=%async_computation.2 | async-start | bytes 1863680 | tf_op jit(solution)/shard_map/all_gather | solution.py:29
  12.2 0.6 copy-start.8
  12.9 207.3 %reduce-scatter.2.cloned.1.call-start = ((), (), s32[]{:S(2)}) async-start(), calls=%async_computation.1 | async-start | bytes 1179648 | tf_op jit(solution)/shard_map/reduce_scatter | solution.py:70
  152.8 4.3 %copy-start.6 = (bf16[64,1024]{1,0:T(8,128)(2,1)S(1)}, bf16[64,1024]{1,0:T(8,128)(2,1)}, u32[]{:S(2)}) copy-start(bf16[64,1024]{1,0:T(8,128)(2,1)} %get-tuple-element.12) | copy-start | bytes 393220
  153.6 4.5 %copy-start.3 = (bf16[1024,128]{1,0:T(8,128)(2,1)S(1)}, bf16[1024,128]{1,0:T(8,128)(2,1)}, u32[]{:S(2)}) copy-start(bf16[1024,128]{1,0:T(8,128)(2,1)} %reshape_reshape.24) | copy-start | bytes 786436
  154.4 3.7 %copy-start.4 = (bf16[1024,128]{1,0:T(8,128)(2,1)S(1)}, bf16[1024,128]{1,0:T(8,128)(2,1)}, u32[]{:S(2)}) copy-start(bf16[1024,128]{1,0:T(8,128)(2,1)} %reshape_reshape.27) | copy-start | bytes 786436
  155.2 2.9 %copy-start.5 = (bf16[1024,128]{1,0:T(8,128)(2,1)S(1)}, bf16[1024,128]{1,0:T(8,128)(2,1)}, u32[]{:S(2)}) copy-start(bf16[1024,128]{1,0:T(8,128)(2,1)} %reshape_reshape.28) | copy-start | bytes 786436
  158.1 2.3 copy-start.2
  160.4 5.0 %copy-start.10 = (f32[3,128]{1,0:T(4,128)S(1)}, f32[3,128]{1,0:T(4,128)}, u32[]{:S(2)}) copy-start(f32[3,128]{1,0:T(4,128)} %param.25) | copy-start | bytes 4612
  160.4 5.0 %copy-start.1 = (bf16[64,2048]{1,0:T(8,128)(2,1)S(1)}, bf16[64,2048]{1,0:T(8,128)(2,1)}, u32[]{:S(2)}) copy-start(bf16[64,2048]{1,0:T(8,128)(2,1)} %get-tuple-element.13) | copy-start | bytes 786436
  160.4 5.9 %copy-start = (bf16[64,2048]{1,0:T(8,128)(2,1)S(1)}, bf16[64,2048]{1,0:T(8,128)(2,1)}, u32[]{:S(2)}) copy-start(bf16[64,2048]{1,0:T(8,128)(2,1)} %get-tuple-element.14) | copy-start | bytes 786436
  161.7 7.1 %copy-start.9 = (pred[128,256]{0,1:T(8,128)(4,1)S(1)}, pred[128,256]{0,1:T(8,128)(4,1)}, u32[]{:S(2)}) copy-start(pred[128,256]{0,1:T(8,128)(4,1)} %fusion.7) | copy-start | bytes 98308
  161.8 5.6 %collective-permute-start = (bf16[64,256]{1,0:T(8,128)(2,1)S(1)}, bf16[64,256]{1,0:T(8,128)(2,1)S(1)}, u32[]{:S(2)}, u32[]{:S(2)}) collective-permute-start(bf16[64,256]{1,0:T(8,128)(2,1)S(1)} %get-tuple-element.19), channel_id=1, source_target_pairs={{0,8},{8,16},{16,24},{24,32},{32,40},{40,48},{48,56},{56,64},{64,7... | collective-permute-start | bytes 98312 | tf_op jit(solution)/shard_map/ppermute | solution.py:62
  164.1 4.7 %collective-permute-start.1 = (bf16[64,256]{1,0:T(8,128)(2,1)S(1)}, bf16[64,256]{1,0:T(8,128)(2,1)S(1)}, u32[]{:S(2)}, u32[]{:S(2)}) collective-permute-start(bf16[64,256]{1,0:T(8,128)(2,1)S(1)} %get-tuple-element.20), channel_id=1, source_target_pairs={{8,0},{16,8},{24,16},{32,24},{40,32},{48,40},{56,48},{64,56},{72,6... | collective-permute-start | bytes 98312 | tf_op jit(solution)/shard_map/ppermute | solution.py:63
  165.5 3.6 %copy-start.12 = (f32[2]{0:T(128)S(1)}, f32[2]{0:T(128)}, u32[]{:S(2)}) copy-start(f32[2]{0:T(128)} %param.24) | copy-start | bytes 28
Sparse Core Ops, SparseCore 0:
  13.0 136.2 all-gather.5
  171.3 48.8 reduce-scatter.1
where the time goes:
time: 230 us; the launch traced here: 229 us
  blocking collectives  132 us (57%)
  waiting for transfers between devices  51.1 us (22%)
  local copies, waits for them, and re-layouts  22.2 us (10%)
  between operations  13.7 us (6%)
  other arithmetic  3.86 us (2%)
  starting transfers between devices  3.71 us (2%)
    all_gather x1, blocking collectives, gather_packed(): lines, at, finished = (lax.all_gather(flat, axis), 0, [])  84 us
    reduce_scatter x1, waiting for transfers between devices, scattered(): lax.psum_scatter(portion(jnp.int32(0), count), axis, scatter_dimension=0,...  49 us
    all_gather x1, blocking collectives, gathered_total(): blocks = lax.all_gather(shard, axis)  34.9 us
    all_gather x2, blocking collectives, gather_axes(): shard = lax.all_gather(shard, axis, axis=dim, tiled=True)  12.8 us
    unnamed x35, local copies, waits for them, and re-layouts  5.75 us
    another operation x8, local copies, waits for them, and re-layouts, joined_along(): blocks.reshape(*lengths[:dim], lengths[dim] * lengths[dim + 1], *lengths[...  5.34 us
  transfers between devices with their start and end apart: 4, of which 3 were waited for; matrix products, arithmetic and copies ran while one was open for 3% of the time, Pallas kernels for 0%

commit v1 on v0

v1 whole, which is shorter than its diff:
```python
import jax
import jax.numpy as jnp
from jax import lax
from jax.experimental import pallas as pl
from jax.experimental.pallas import tpu as pltpu
from jax.sharding import Mesh
from jax.sharding import PartitionSpec as P

MESH = pl.DeviceIdType.MESH
NZ, NY, NX = 16, 4, 4
TOK = 128
ROWS = NY * TOK
HALO = 64
SEQ = NZ * ROWS
EPS = 1e-06
NEG = -1e30
F32 = jnp.float32
BF16 = jnp.bfloat16


def lanes(shape):
    return lax.broadcasted_iota(jnp.int32, shape, len(shape) - 1)


def swap(v):
    return pltpu.roll(v, 64, v.ndim - 1)


def fold(v):
    low, high = v[: v.shape[0] // 2], v[v.shape[0] // 2 :]
    return jnp.where(lanes(low.shape) < 64, swap(low), high)


def unfold(a, b):
    first = lanes(a.shape) < 64
    return jnp.where(first, a, swap(b)), jnp.where(first, swap(a), b)


def kernel(
    tokens, gain, wq, wk, wv, wci, wpre, wpost, wag, wcg, sink, taps, wao, wco,
    out,
    tok, par, w, ow, normed, kv, qp, gsend, grecv, asend, arecv, left, xsend, xrecv,
    raw, rawk, rawv, rawo, rawg, rawt, raws, pack, opack,
    load_sem, a_send, a_recv, t_send, tx_recv, ty_recv, td_recv, p_send, px_recv, pd_recv,
    w_send, w_recv, o1_send, o1_recv, o2_send, o2_recv, o3_send, o3_recv,
    h_send, h_recv, g_send, g_recv, e_send, e_recv, d_send, d_recv,
):
    z, y, x, c = (lax.axis_index(n) for n in ("z", "y", "x", "c"))

    def at(dz=0, ny=None, nx=None, nc=None):
        return (
            lax.rem(z + dz + NZ, NZ) if dz else z,
            y if ny is None else ny,
            x if nx is None else nx,
            c if nc is None else nc,
        )

    ys = [lax.rem(y + d, NY) for d in (1, 2, 3)]
    xs = [lax.rem(x + d, NX) for d in (1, 2, 3)]
    other = 1 - c

    barrier = pltpu.get_barrier_semaphore()
    peers = [at(dz=d) for d in (-2, -1, 1, 2)] + [at(nc=other)]
    peers += [at(ny=n, nc=m) for n in ys for m in (c, other)]
    peers += [at(nx=n, nc=m) for n in xs for m in (c, other)]
    for peer in peers:
        pl.semaphore_signal(barrier, inc=1, device_id=peer, device_id_type=MESH)

    loads = []

    def load(src, dst):
        copy = pltpu.make_async_copy(src, dst, load_sem.at[len(loads)])
        copy.start()
        loads.append(copy)

    for k, ref in enumerate((wq, wag, wci, wcg, wpre, wpost)):
        load(ref, raw.at[k])
    load(wk, rawk)
    load(wv, rawv)
    load(gain, rawg)
    load(taps, rawt)
    load(sink, raws)
    load(tokens, tok.at[y, c, x])
    load(wao, rawo.at[0])
    load(wco, rawo.at[1])
    for copy in loads:
        copy.wait()

    q32, ag32, ci32, cg32, pre32, post32 = (raw[k].astype(F32) for k in range(6))
    first = lanes((16, 128)) < 64
    kv32 = jnp.concatenate([rawk[...].astype(F32), rawv[...].astype(F32)], axis=1)

    def joined(a, b, half):
        return jnp.where(first, a, swap(b)) if half == 0 else jnp.where(first, swap(a), b)

    for b in range(2):
        pack[b, 0, :, :128] = joined(q32, ag32, b).astype(BF16)
        pack[b, 0, :, 128:] = kv32.astype(BF16)
        pack[b, 1, :, :128] = joined(ci32, cg32, b).astype(BF16)
        pack[b, 1, :, 128:] = joined(pre32, post32, b).astype(BF16)
    for m in range(2):
        opack[m] = rawo[m].astype(F32).T.astype(BF16)
    par[c, x] = jnp.zeros((8, 128), F32)
    par[c, x, 0:1, :] = rawg[...]
    par[c, x, 1:4, :] = rawt[...]
    par[c, x, 4:5, 0:2] = raws[...]

    pl.semaphore_wait(barrier, len(peers))

    ends = []

    def send(src, dst, send_sem, recv_sem, device, when=None):
        copy = pltpu.make_async_remote_copy(
            src_ref=src, dst_ref=dst, send_sem=send_sem, recv_sem=recv_sem, device_id=device, device_id_type=MESH
        )
        if when is None:
            copy.start()
        else:
            pl.when(when)(copy.start)
        ends.append((copy, when))

    def arrived(ref, sem):
        pltpu.make_async_copy(ref, ref, sem).wait()

    for b in range(2):
        for m in range(2):
            mine = jnp.logical_and(2 * c + b == y, c == m)
            send(
                pack.at[b, m], w.at[z, y], a_send.at[2 * b + m], a_recv,
                at(ny=2 * c + b, nc=m), jnp.logical_not(mine),
            )

            @pl.when(mine)
            def _():
                w[z, y] = pack[b, m]

    for k, n in enumerate(xs):
        send(tok.at[y, c, x], tok.at[y, c, x], t_send.at[k], tx_recv, at(nx=n))
        send(par.at[c, x], par.at[c, x], p_send.at[k], px_recv, at(nx=n))

    relay = z // 4
    for m in range(2):
        mine = jnp.logical_and(x == relay, c == m)
        spot = ow.at[z % 4, y, :, pl.ds(pl.multiple_of((2 * x + c) * 128, 128), 128)]
        send(opack.at[m], spot, o1_send.at[m], o1_recv, at(nx=relay, nc=m), jnp.logical_not(mine))

        @pl.when(mine)
        def _():
            ow[z % 4, y, :, pl.ds(pl.multiple_of((2 * x + c) * 128, 128), 128)] = opack[m]

    own_piece = (y // 2) == c

    @pl.when(own_piece)
    def _():
        arrived(w.at[z, 0:3], a_recv)

    @pl.when(jnp.logical_not(own_piece))
    def _():
        arrived(w.at[z], a_recv)

    def w_block(d):
        return w.at[lax.rem(z - d + NZ, NZ)]

    def w_index(d):
        return d - 1 if d > 0 else 7 - d

    def w_pass(d, hop):
        block = w_block(d)
        send(block, block, w_send.at[w_index(d + hop)], w_recv.at[w_index(d + hop)], at(dz=hop))

    def o_block(d):
        source = lax.rem(z - d + NZ, NZ)
        return (source // 4) == x, lax.rem(source, 4)

    def o_pass(d, hops):
        here, zi = o_block(d)
        block = ow.at[zi, y]
        if d != 0:
            pl.when(here)(lambda: arrived(block, o2_recv.at[zi]))
        for hop in hops:
            spot = {1: 0, 2: 1, -1: 2, -2: 3}[hop]
            send(block, block, o2_send.at[w_index(d + hop)], o2_recv.at[zi], at(dz=hop), here)
        for k, n in enumerate(ys):
            send(block, block, o3_send.at[8 + d, k], o3_recv, at(ny=n), here)

    for hop in (2, -2, 1, -1):
        w_pass(0, hop)

    @pl.when(x == relay)
    def _():
        arrived(ow.at[z % 4, y, :, 0:896], o1_recv)

    o_pass(0, (2, -2, 1, -1))

    arrived(tok.at[y, c, 0:3], tx_recv)
    for k, n in enumerate(ys):
        send(tok.at[y, c], tok.at[y, c], t_send.at[3 + k], ty_recv.at[k], at(ny=n))
    arrived(par.at[c, 0:3], px_recv)
    send(par.at[c], par.at[c], p_send.at[3], pd_recv, at(nc=other))
    send(tok.at[y, c], tok.at[y, c], t_send.at[6], td_recv, at(nc=other))

    for k in (1, 2, 3):
        for d in (2 * k, -2 * k):
            arrived(w_block(d), w_recv.at[w_index(d)])
            for hop in (2, 1) if d > 0 else ((-2, -1) if k < 3 else (-1,)):
                w_pass(d, hop)
        for d in (2 * k - 1, 1 - 2 * k):
            o_pass(d, ())
        for d in (2 * k, -2 * k):
            o_pass(d, (2, 1) if d > 0 else ((-2, -1) if k < 3 else (-1,)))
        if k == 2:
            for j in range(3):
                rows = tok.at[lax.rem(y - j - 1 + NY, NY), c]
                arrived(rows, ty_recv.at[j])
                send(rows, rows, t_send.at[7 + j], td_recv, at(nc=other))
    arrived(tok.at[:, other], td_recv)
    arrived(par.at[other], pd_recv)

    def normalise(i, _):
        total = jnp.zeros((TOK, 128), F32)
        for m in range(2):
            for n in range(NX):
                v = tok[i, m, n].astype(F32)
                total += v * v
        scale = lax.rsqrt(jnp.sum(total, axis=1, keepdims=True) / 1024 + EPS)
        rows = pl.ds(pl.multiple_of(i * TOK, TOK), TOK)
        for m in range(2):
            for n in range(NX):
                v = tok[i, m, n].astype(F32) * scale * par[m, n, 0:1, :]
                t = 128 * (2 * n + m)
                normed[rows, t : t + 128] = v.astype(BF16)
        return 0

    lax.fori_loop(0, NY, normalise, 0)

    for d in (1, -1, 3, -3, 5, -5, 7, -7, 8):
        arrived(w_block(d), w_recv.at[w_index(d)])

    weights = w[...].reshape(1024, 256)
    half = lanes((TOK, 128)) < 64
    for i in range(NY):
        rows = slice(i * TOK, i * TOK + TOK)
        spot = slice(HALO + i * TOK, HALO + i * TOK + TOK)
        result = jnp.dot(normed[rows, :], weights, preferred_element_type=F32)
        one, two = result[:, :128], result[:, 128:]
        two_b = two.astype(BF16)

        @pl.when(c == 0)
        def _():
            kv[spot, :] = two_b
            qp[rows, :] = jnp.where(half, one, 0.0).astype(BF16)

        @pl.when(c == 1)
        def _():
            mix = one.astype(BF16).astype(F32) * two_b.astype(F32)
            kv[spot, :] = swap(mix).astype(BF16)
            qp[rows, :] = two_b

        gsend[i] = fold(jax.nn.sigmoid(one))

    for k, hop in enumerate((1, -1)):
        src = kv.at[ROWS : ROWS + HALO] if hop == 1 else kv.at[HALO : 2 * HALO]
        dst = kv.at[0:HALO] if hop == 1 else kv.at[ROWS + HALO : ROWS + 2 * HALO]
        send(src, dst, h_send.at[k], h_recv.at[k], at(dz=hop))
    for k, n in enumerate(ys):
        send(gsend.at[n], grecv.at[y], g_send.at[k], g_recv, at(ny=n))
    grecv[y] = gsend[y]

    for d in (7, -7, 8):
        o_pass(d, ())

    small = par[y // 2, x]
    sink_here = jnp.sum(jnp.where(lanes((1, 128)) == lax.rem(y, 2), small[4:5, :], 0.0), axis=1, keepdims=True)
    tap_rows = jnp.where(lax.rem(y, 2) == 1, small, swap(small))

    def attend(i):
        q = qp[i * TOK : i * TOK + TOK, :]
        keys = kv[i * TOK : i * TOK + TOK + 2 * HALO, :]
        s = lax.dot_general(q, keys, (((1,), (1,)), ((), ())), preferred_element_type=F32) * 0.125
        gap = lanes(s.shape) - lax.broadcasted_iota(jnp.int32, s.shape, 0)
        place = z * ROWS + (i * TOK - HALO) + lanes(s.shape)
        allowed = (gap >= 0) & (gap <= 2 * HALO) & (place >= 0) & (place < SEQ)
        s = jnp.where(allowed, s, NEG)
        top = jnp.maximum(jnp.max(s, axis=1, keepdims=True), sink_here)
        p = jnp.exp(s - top)
        total = jnp.sum(p, axis=1, keepdims=True) + jnp.exp(sink_here - top)
        high = p.astype(BF16)
        low = (p - high.astype(F32)).astype(BF16)
        mixed = jnp.dot(high, keys, preferred_element_type=F32) + jnp.dot(low, keys, preferred_element_type=F32)
        asend[i] = fold(mixed / total).astype(BF16)

    def convolve(i):
        wide = kv[HALO - 16 + i * TOK : HALO + 16 + i * TOK + TOK, :].astype(F32)
        size = wide.shape[0]
        before = pltpu.roll(wide, 1, 0)[16 : 16 + TOK]
        after = pltpu.roll(wide, size - 1, 0)[16 : 16 + TOK]
        place = z * ROWS + i * TOK + lax.broadcasted_iota(jnp.int32, before.shape, 0)
        before = jnp.where(place == 0, 0.0, before)
        after = jnp.where(place == SEQ - 1, 0.0, after)
        total = tap_rows[1:2] * before + tap_rows[2:3] * wide[16 : 16 + TOK] + tap_rows[3:4] * after
        asend[i] = fold(qp[i * TOK : i * TOK + TOK, :].astype(F32) * total).astype(BF16)

    for step, i in enumerate((1, 2, 0, 3)):
        if i == 0:
            arrived(kv.at[0:HALO], h_recv.at[0])
        if i == 3:
            arrived(kv.at[ROWS + HALO : ROWS + 2 * HALO], h_recv.at[1])
        pl.when(c == 0)(lambda: attend(i))
        pl.when(c == 1)(lambda: convolve(i))
        for n in range(NX):
            mine = jnp.logical_and(y == i, x == n)
            send(
                asend.at[i], arecv.at[4 * x + y], e_send.at[4 * i + n], e_recv,
                at(ny=i, nx=n), jnp.logical_not(mine),
            )
    arecv[4 * x + y] = asend[y]

    arrived(ow.at[0:3], o3_recv)
    arrived(grecv.at[0:3], g_recv)
    arrived(arecv.at[0:15], e_recv)
    for j in range(8):
        low, high = unfold(arecv[2 * j].astype(F32), arecv[2 * j + 1].astype(F32))
        left[0:64, 128 * j : 128 * j + 128] = low.astype(BF16)
        left[64:128, 128 * j : 128 * j + 128] = high.astype(BF16)
    branch = lax.dot_general(
        left[...], ow[...].reshape(256, 1024), (((1,), (1,)), ((), ())), preferred_element_type=F32
    )
    parts = []
    for j in range(2):
        low, high = unfold(grecv[2 * j], grecv[2 * j + 1])
        parts.append(branch[:, 128 * j : 128 * j + 128] * jnp.concatenate([low, high], axis=0))
    xsend[...] = jnp.where(c == 0, parts[1], parts[0])
    send(xsend, xrecv, d_send, d_recv, at(nc=other))
    kept = jnp.where(c == 0, parts[0], parts[1])
    arrived(xrecv, d_recv)
    out[...] = (kept + xrecv[...]).astype(BF16)

    for copy, when in ends:
        if when is None:
            copy.wait_send()
        else:
            pl.when(when)(copy.wait_send)


def on_device(
    tokens, norm_gain, query_weight, key_weight, value_weight, conv_in_weight, pre_weight, post_weight,
    attn_gate_weight, conv_gate_weight, sink_logit, conv_taps, attn_out_weight, conv_out_weight,
):
    dma = pltpu.SemaphoreType.DMA
    vmem = pltpu.VMEM
    return pl.pallas_call(
        kernel,
        out_shape=jax.ShapeDtypeStruct((TOK, 128), BF16),
        in_specs=[pl.BlockSpec(memory_space=pl.ANY)] * 14,
        out_specs=pl.BlockSpec(memory_space=pltpu.VMEM),
        scratch_shapes=[
            vmem((NY, 2, NX, TOK, 128), BF16),
            vmem((2, NX, 8, 128), F32),
            vmem((NZ, NY, 16, 256), BF16),
            vmem((4, NY, 16, 1024), BF16),
            vmem((ROWS, 1024), BF16),
            vmem((ROWS + 2 * HALO, 128), BF16),
            vmem((ROWS, 128), BF16),
            vmem((NY, 64, 128), F32),
            vmem((NY, 64, 128), F32),
            vmem((NY, 64, 128), BF16),
            vmem((NX * NY, 64, 128), BF16),
            vmem((TOK, 1024), BF16),
            vmem((TOK, 128), F32),
            vmem((TOK, 128), F32),
            vmem((6, 16, 128), BF16),
            vmem((16, 64), BF16),
            vmem((16, 64), BF16),
            vmem((2, 128, 16), BF16),
            vmem((1, 128), F32),
            vmem((3, 128), F32),
            vmem((1, 2), F32),
            vmem((2, 2, 16, 256), BF16),
            vmem((2, 16, 128), BF16),
            dma((14,)),
            dma((4,)), dma,
            dma((10,)), dma, dma((3,)), dma,
            dma((4,)), dma, dma,
            dma((15,)), dma((15,)),
            dma((2,)), dma,
            dma((15,)), dma((4,)),
            dma((17, 3)), dma,
            dma((2,)), dma((2,)),
            dma((3,)), dma,
            dma((16,)), dma,
            dma, dma,
        ],
        compiler_params=pltpu.CompilerParams(collective_id=0, has_side_effects=True, vmem_limit_bytes=48 << 20),
    )(
        tokens, norm_gain.reshape(1, 128), query_weight, key_weight, value_weight, conv_in_weight, pre_weight,
        post_weight, attn_gate_weight, conv_gate_weight, sink_logit.reshape(1, 2), conv_taps, attn_out_weight,
        conv_out_weight,
    )


def solution(mesh):
    fine = Mesh(mesh.devices.reshape(NZ, NY, NX, 2), ("z", "y", "x", "c"))
    sp, tp = ("z", "y"), ("x", "c")
    return jax.shard_map(
        on_device,
        mesh=fine,
        in_specs=(P(sp, tp), P(tp)) + (P(sp, tp),) * 8 + (P(tp), P(None, tp), P(tp, sp), P(tp, sp)),
        out_specs=P(sp, tp),
        check_vma=False,
    )
```

time: 230 us -> 50.3 us (0.22)
  blocking collectives: 132 us -> 0 us
  waiting for transfers between devices: 51.1 us -> 0 us
  Pallas kernels: 0 us -> 47.9 us
  local copies, waits for them, and re-layouts: 22.2 us -> 2.17 us
  between operations: 13.7 us -> 0.1 us
  other arithmetic: 3.86 us -> 0 us
  starting transfers between devices: 3.71 us -> 0 us
    all_gather x4 -> x0, blocking collectives: 132 us -> none  [the longest x1 84 us: gather_packed(): lines, at, finished = (lax.all_gather(flat, axis), 0, [])]
    reduce_scatter x1 -> x0, waiting for transfers between devices: 49 us -> none  [scattered(): lax.psum_scatter(portion(jnp.int32(0), count), axis, scatter_dimension=0,...]
    pallas_call x0 -> x1, Pallas kernels: none -> 47.9 us  [on_device(): pl.pallas_call(kernel, out_shape=jax.ShapeDtypeStruct((TOK, 128), BF16),...]
    another operation x8 -> x0, local copies, waits for them, and re-layouts: 5.34 us -> none  [joined_along(): blocks.reshape(*lengths[:dim], lengths[dim] * lengths[dim + 1], *lengths[...]
    ppermute x2 -> x0, starting transfers between devices: 3.66 us -> none  [the longest x1 2.37 us: padded_2(): before = lax.ppermute(last, axis, up)]
    unnamed x35 -> x29, local copies, waits for them, and re-layouts: 5.75 us -> 2.17 us
    concatenate x2 -> x0, local copies, waits for them, and re-layouts: 2.95 us -> none  [the longest x1 2.26 us: on_device(): stacked = jnp.concatenate(collected, axis=1)]
    all_gather x2 -> x0, local copies, waits for them, and re-layouts: 2.86 us -> none  [gather_packed(): lines, at, finished = (lax.all_gather(flat, axis), 0, [])]
  transfers between devices with their start and end apart: 4 -> 0, of which waited for: 3 -> 0; matrix products, arithmetic and copies ran while one was open for 3% -> 0% of each run, Pallas kernels for 0% -> 0%
where the time goes in v1:
time: 50.3 us; the launch traced here: 50.1 us
  Pallas kernels  47.9 us (95%)
  local copies, waits for them, and re-layouts  2.17 us (4%)
    pallas_call x1, Pallas kernels, on_device(): pl.pallas_call(kernel, out_shape=jax.ShapeDtypeStruct((TOK, 128), BF16),...  47.9 us
    unnamed x29, local copies, waits for them, and re-layouts  2.17 us

profile of v1, /device:TPU:1, one launch (start us, length us, event | category | flops | bytes accessed | tf_op | source)
XLA Modules:
  0.0 50.1 jit_solution(5824154138932540650)
XLA Ops:
  0.0 0.0 copy-start.12
  0.0 0.0 copy-start
  0.0 0.8 %copy.15.wao = bf16[128,16]{1,0:T(8,128)(2,1)S(1)} copy(bf16[128,16]{0,1:T(8,128)(2,1)} %param.26) | data formatting | bytes 8192 | tf_op args[12]
  0.8 0.0 copy-done.12
  0.8 0.0 copy-start.1
  0.8 0.0 copy-start.2
  0.8 0.0 copy-start.3
  0.9 0.0 copy-start.4
  0.9 0.0 copy-start.5
  0.9 0.0 copy-start.6
  0.9 0.0 copy-start.7
  0.9 0.0 copy-start.8
  0.9 0.0 copy-start.9
  0.9 0.0 copy-start.10
  0.9 0.0 copy-start.11
  1.0 0.1 copy.16.wco
  1.1 0.0 copy-done
  1.1 0.4 copy-done.1
  1.5 0.0 copy-done.2
  1.5 0.0 copy-done.3
  1.6 0.0 copy-done.4
  1.6 0.0 copy-done.5
  1.6 0.0 copy-done.6
  1.6 0.0 copy-done.7
  1.6 0.0 copy-done.8
  1.6 0.0 copy-done.9
  1.6 0.0 copy-done.10
  1.6 0.0 copy-done.11
  1.6 47.9 %shard_map.136 = bf16[128,128]{1,0:T(8,128)(2,1)S(1)} custom-call(bf16[128,128]{1,0:T(8,128)(2,1)S(1)} %copy-done, f32[1,128]{1,0:T(1,128)S(1)} %bitcast.2, bf16[16,128]{1,0:T(8,128)(2,1)S(1)} %copy-done.1, bf16[16,64]{1,0:T(8,128)(2,1)S(1)} %copy-done.2, bf16[16,64]{1,0:T(8,128)(2,1)S(1)} %copy-done.3, bf16[16,128]{1,0:T(8,128)(2,1)S(1)} %copy-done.4, ...), custom_call_target="tpu_custom_call" | custom-call | tf_op jit(solution)/shard_map/pallas_call | solution.py:351
  49.5 0.6 %copy.18 = bf16[128,128]{1,0:T(8,128)(2,1)} copy(bf16[128,128]{1,0:T(8,128)(2,1)S(1)} %shard_map.136) | data formatting | bytes 65536
Async XLA Ops:
  0.0 0.8 %copy-start.12 = (bf16[128,16]{0,1:T(8,128)(2,1)S(1)}, bf16[128,16]{0,1:T(8,128)(2,1)}, u32[]{:S(2)}) copy-start(bf16[128,16]{0,1:T(8,128)(2,1)} %param.27) | copy-start | bytes 12292
  0.0 1.1 %copy-start = (bf16[128,128]{1,0:T(8,128)(2,1)S(1)}, bf16[128,128]{1,0:T(8,128)(2,1)}, u32[]{:S(2)}) copy-start(bf16[128,128]{1,0:T(8,128)(2,1)} %tokens.1) | copy-start | bytes 98308
  0.8 0.7 %copy-start.1 = (bf16[16,128]{1,0:T(8,128)(2,1)S(1)}, bf16[16,128]{1,0:T(8,128)(2,1)}, u32[]{:S(2)}) copy-start(bf16[16,128]{1,0:T(8,128)(2,1)} %wq.1) | copy-start | bytes 12292
  0.8 0.7 %copy-start.2 = (bf16[16,64]{1,0:T(8,128)(2,1)S(1)}, bf16[16,64]{1,0:T(8,128)(2,1)}, u32[]{:S(2)}) copy-start(bf16[16,64]{1,0:T(8,128)(2,1)} %wk.1) | copy-start | bytes 6148
  0.8 0.7 %copy-start.3 = (bf16[16,64]{1,0:T(8,128)(2,1)S(1)}, bf16[16,64]{1,0:T(8,128)(2,1)}, u32[]{:S(2)}) copy-start(bf16[16,64]{1,0:T(8,128)(2,1)} %wv.1) | copy-start | bytes 6148
  0.9 0.7 %copy-start.4 = (bf16[16,128]{1,0:T(8,128)(2,1)S(1)}, bf16[16,128]{1,0:T(8,128)(2,1)}, u32[]{:S(2)}) copy-start(bf16[16,128]{1,0:T(8,128)(2,1)} %wci.1) | copy-start | bytes 12292
  0.9 0.7 %copy-start.5 = (bf16[16,128]{1,0:T(8,128)(2,1)S(1)}, bf16[16,128]{1,0:T(8,128)(2,1)}, u32[]{:S(2)}) copy-start(bf16[16,128]{1,0:T(8,128)(2,1)} %wpre.1) | copy-start | bytes 12292
  0.9 0.7 %copy-start.6 = (bf16[16,128]{1,0:T(8,128)(2,1)S(1)}, bf16[16,128]{1,0:T(8,128)(2,1)}, u32[]{:S(2)}) copy-start(bf16[16,128]{1,0:T(8,128)(2,1)} %wpost.1) | copy-start | bytes 12292
  0.9 0.7 %copy-start.7 = (bf16[16,128]{1,0:T(8,128)(2,1)S(1)}, bf16[16,128]{1,0:T(8,128)(2,1)}, u32[]{:S(2)}) copy-start(bf16[16,128]{1,0:T(8,128)(2,1)} %wag.1) | copy-start | bytes 12292
  0.9 0.7 %copy-start.8 = (bf16[16,128]{1,0:T(8,128)(2,1)S(1)}, bf16[16,128]{1,0:T(8,128)(2,1)}, u32[]{:S(2)}) copy-start(bf16[16,128]{1,0:T(8,128)(2,1)} %wcg.1) | copy-start | bytes 12292
  0.9 0.7 %copy-start.9 = (f32[3,128]{1,0:T(4,128)S(1)}, f32[3,128]{1,0:T(4,128)}, u32[]{:S(2)}) copy-start(f32[3,128]{1,0:T(4,128)} %taps.1) | copy-start | bytes 4612
  0.9 0.7 %copy-start.10 = (f32[128]{0:T(128)S(1)}, f32[128]{0:T(128)}, u32[]{:S(2)}) copy-start(f32[128]{0:T(128)} %param.15) | copy-start | bytes 1540
  0.9 0.7 %copy-start.11 = (f32[2]{0:T(128)S(1)}, f32[2]{0:T(128)}, u32[]{:S(2)}) copy-start(f32[2]{0:T(128)} %param.24) | copy-start | bytes 28
